TPU v7x, 512 devices: a whole 4x8x8 slice. The times are simulated.
512 devices in a mesh: ep: 32 (over z, x), tp: 16 (over y, core).
Axes of the slice: x: 4, y: 8, z: 8, core: 2. Of those that a mesh axis runs over, the one named last changes fastest.
Arguments:
- mix_query: bfloat16 [8192, 2048], P('ep', 'tp'), may hold values from -6 to 6
- forget_input: bfloat16 [8192, 2048], P('ep', 'tp'), may hold values from -6 to 6
- mix_value: bfloat16 [8192, 2048], P('ep', 'tp'), may hold values from -6 to 6
- out_gate_input: bfloat16 [8192, 2048], P('ep', 'tp'), may hold values from -6 to 6
- decay_shift: float32 [8192, 16], P('ep', 'tp'), may hold values from -1.5 to 0
- forget_floor: float32 [2048], P('tp'), may hold values from 0.9 to 1
- head_gain: float32 [128], replicated, may hold values from 0.1 to 1.9
- w_mix_out: bfloat16 [2048, 2048], P(None, 'tp'), may hold values from -0.125 to 0.125
- moe_input: bfloat16 [8192, 2048], P('ep'), may hold values from -6 to 6
- moe_gain: float32 [2048], replicated, may hold values from 0.1 to 1.9
- routes: int32 [8192, 2], P('ep'), may hold values from 0 to 31, all different within a row; in each aligned block of 256 rows (0 to 255, 256 to 511, ...) at most 20 rows name the same one
- route_weight: float32 [8192, 2], P('ep'), may hold values from 0.1 to 1
- w_exp_gate: bfloat16 [32, 2048, 4096], P('ep', None, 'tp'), may hold values from -0.125 to 0.125
- w_exp_up: bfloat16 [32, 2048, 4096], P('ep', None, 'tp'), may hold values from -0.125 to 0.125
- w_exp_down: bfloat16 [32, 4096, 2048], P('ep', 'tp'), may hold values from -0.125 to 0.125
Outputs:
- mixed: bfloat16 [8192, 2048], P('ep', 'tp')
- moe_out: bfloat16 [8192, 2048], P('ep', 'tp')
Inputs may be any that keep to these rules, and one draw needn't show every extreme that they name: `routes`: at most 20 of the rows of one index of ep name one expert, and in every draw some device's rows name one expert exactly 20 times; the experts of a row differ.
All inputs are finite; a program needn't handle non-finite values.
Results may differ from a plain program's by a relative error of at most 0.02.
Values may be sent and summed in bfloat16 or wider, within the bound.
A program may use at most 64 MiB of HBM per device.

v0:
```python
import jax
import jax.numpy as jnp
from jax import lax
from jax.sharding import Mesh
from jax.sharding import PartitionSpec as P

TOP_K = 2
EP = ("ep_0", "ep_1")
TP = ("tp_0", "tp_1")
eps = 1e-06
highest_precision = lax.Precision.HIGHEST


def nothing_yet(shard, identity):
    return jax.tree.map(
        lambda a, e: jnp.broadcast_to(jnp.asarray(e, a.dtype), a.shape), shard, identity
    )


def gathered_once(shard, axis):
    leaves = jax.tree.leaves(shard)
    sequence = sorted(range(len(leaves)), key=lambda k: -leaves[k].size)
    width = (1, *leaves[sequence[0]].shape)[-1]
    lines = [
        jnp.pad(leaves[k].reshape(-1), (0, -leaves[k].size % width)).reshape(-1, width)
        for k in sequence
    ]
    both, at, found = (lax.all_gather(jnp.concatenate(lines), axis), 0, {})
    for k, line in zip(sequence, lines):
        slab = both[:, at : at + len(line)].reshape(len(both), -1)
        found[k] = slab[:, : leaves[k].size].reshape(-1, *leaves[k].shape)
        at += len(line)
    numbers = iter(range(len(leaves)))
    return jax.tree.map(lambda _: found[next(numbers)], shard)


def carried_in(shard, axes, combine, identity):
    before = start = nothing_yet(shard, identity)
    running = shard
    for axis in reversed(axes):
        peers, index = (lax.axis_size(axis), lax.axis_index(axis))
        pieces = gathered_once(
            jax.tree.map(
                lambda part, kind: part.astype(kind), running, (jnp.bfloat16, jnp.bfloat16)
            ),
            axis,
        )
        inside, running = (start, start)
        for k in range(peers):
            passed = k < index
            running = combine(
                running, jax.tree.map(lambda part, own: part[k].astype(own.dtype), pieces, shard)
            )
            inside = jax.tree.map(lambda new, old: jnp.where(passed, new, old), running, inside)
        before = combine(inside, before)
    return before


def sent_to_all(shard, axis):
    peers = lax.axis_size(axis)
    return lax.all_to_all(
        jnp.broadcast_to(shard[None], (peers, *shard.shape)), axis, 0, 0, tiled=True
    )


def laid_out(tiles, dim):
    tiles = jnp.moveaxis(tiles, 0, dim)
    lengths = tiles.shape
    return tiles.reshape(*lengths[:dim], lengths[dim] * lengths[dim + 1], *lengths[dim + 2 :])


def gather_directly(shard, axis, dim):
    tiles = sent_to_all(shard, axis)
    return laid_out(tiles, dim)


def split_up(shard, dim, peers):
    lengths = shard.shape
    tiles = shard.reshape(*lengths[:dim], peers, lengths[dim] // peers, *lengths[dim + 1 :])
    return jnp.moveaxis(tiles, dim, 0)


def scatter_pairs(shard, chips, core, dim):
    sizes = (lax.axis_size(chips), lax.axis_size(core))
    tiles = split_up(shard, dim, sizes[0] * sizes[1])
    inside = tiles.shape[1:]
    tiles = tiles.reshape(*sizes, *inside).swapaxes(0, 1).reshape(-1, *inside)
    tiles = lax.psum_scatter(tiles, core, scatter_dimension=0, tiled=True)
    return lax.psum_scatter(tiles, chips, scatter_dimension=0, tiled=True)[0]


def chain_step(earlier, later):
    return (earlier[0] * later[0], later[0][:, :, None] * earlier[1] + later[1])


def token_mixer(
    mix_query,
    forget_input,
    mix_value,
    out_gate_input,
    decay_shift,
    forget_floor,
    head_gain,
    w_mix_out,
):
    length = mix_query.shape[0]
    heads_here = decay_shift.shape[1]
    head_size = head_gain.shape[0]
    gate_input = forget_input.astype(jnp.float32)
    forget = forget_floor + (1.0 - forget_floor) * jax.nn.sigmoid(gate_input)
    input_gate = (1.0 - forget_floor) * jax.nn.sigmoid(-gate_input)
    log_decay = jnp.log(forget) + jnp.repeat(decay_shift, head_size, axis=1)

    def by_head(array):
        return array.reshape(length, heads_here, head_size).transpose(1, 0, 2)

    running_decay = jnp.cumsum(by_head(log_decay), axis=1)
    query_rows = by_head(mix_query.astype(jnp.float32)) * jnp.exp(running_decay)
    head_keys = by_head(input_gate)
    values = by_head(mix_value.astype(jnp.float32))
    scores = jnp.einsum(
        "htk,hsk->hts", query_rows, head_keys * jnp.exp(-running_decay), precision=highest_precision
    )
    causal = jnp.arange(length)[:, None] >= jnp.arange(length)[None, :]
    scores = jnp.where(causal[None, :, :], scores, 0.0)
    within_block_output = jnp.einsum("hts,hsv->htv", scores, values, precision=highest_precision)
    closing_total = running_decay[:, -1, :]
    carried_over_state = jnp.einsum(
        "gbx,gbi->gxi",
        head_keys * jnp.exp(closing_total[:, None, :] - running_decay),
        values,
        precision=highest_precision,
    )
    incoming_state = carried_in(
        (jnp.exp(closing_total), carried_over_state),
        EP,
        chain_step,
        (jnp.ones_like(closing_total), jnp.zeros_like(carried_over_state)),
    )[1]
    block_result = within_block_output + jnp.einsum(
        "rsd,rda->rsa", query_rows, incoming_state, precision=highest_precision
    )
    inverse = lax.rsqrt(jnp.mean(block_result * block_result, axis=2, keepdims=True) + eps)
    gated = by_head(jax.nn.silu(out_gate_input.astype(jnp.float32)))
    normed_heads = (block_result * inverse * head_gain * gated).transpose(1, 0, 2)
    head_out = normed_heads.reshape(length, heads_here * head_size).astype(jnp.bfloat16)
    mixed = jnp.dot(
        lax.all_gather(head_out, TP, axis=1, tiled=True),
        w_mix_out,
        preferred_element_type=jnp.float32,
    )
    return mixed.astype(jnp.bfloat16)


def experts_layer(moe_input, moe_gain, routes, route_weight, w_exp_gate, w_exp_up, w_exp_down):
    row_count = moe_input.shape[0]
    expert_count = lax.axis_size(EP)
    capacity = 5 * row_count * TOP_K // (4 * expert_count)
    token_rows = moe_input.astype(jnp.float32)
    inverse = lax.rsqrt(jnp.mean(token_rows * token_rows, axis=1, keepdims=True) + eps)
    normed = (token_rows * inverse * moe_gain).astype(jnp.bfloat16)
    flat_ids = routes.reshape(-1)
    pair_count = flat_ids.shape[0]
    one_hot = (flat_ids[:, None] == jnp.arange(expert_count, dtype=jnp.int32)[None, :]).astype(
        jnp.int32
    )
    earlier_count = jnp.cumsum(one_hot, axis=0) - one_hot
    ranks = jnp.sum(earlier_count * one_hot, axis=1)
    slot_ids = flat_ids * capacity + ranks
    owners = (
        jnp.zeros((expert_count * capacity,), jnp.int32)
        .at[slot_ids]
        .set(jnp.arange(pair_count, dtype=jnp.int32) // TOP_K)
    )
    filled = (
        jnp.zeros((expert_count * capacity,), jnp.bfloat16)
        .at[slot_ids]
        .set(jnp.ones((pair_count,), jnp.bfloat16))
    )
    outgoing = normed[owners] * filled[:, None]
    w_gate = w_exp_gate[0]
    w_up = w_exp_up[0]
    w_down = w_exp_down[0]
    width = normed.shape[1] // lax.axis_size(TP)
    own_slice = lax.dynamic_slice_in_dim(outgoing, lax.axis_index(TP) * width, width, 1)
    arrived = lax.all_to_all(own_slice, EP, split_axis=0, concat_axis=0, tiled=True)
    portion = gather_directly(arrived, TP, 1)
    gate_sum = jnp.dot(portion, w_gate, preferred_element_type=jnp.float32)
    up_sum = jnp.dot(portion, w_up, preferred_element_type=jnp.float32)
    hidden = (jax.nn.silu(gate_sum) * up_sum).astype(jnp.bfloat16)
    partial_value = jnp.dot(hidden, w_down, preferred_element_type=jnp.float32)
    summed = (
        scatter_pairs(partial_value.astype(jnp.bfloat16), "tp_0", "tp_1", 1)
        .astype(jnp.float32)
        .astype(jnp.bfloat16)
    )
    returned = lax.all_to_all(summed, EP, split_axis=0, concat_axis=0, tiled=True)
    picked = returned[slot_ids].astype(jnp.float32).reshape(row_count, TOP_K, returned.shape[1])
    combined = jnp.sum(picked * route_weight[:, :, None], axis=1)
    return combined.astype(jnp.bfloat16)


def body(
    mix_query,
    forget_input,
    mix_value,
    out_gate_input,
    decay_shift,
    forget_floor,
    head_gain,
    w_mix_out,
    moe_input,
    moe_gain,
    routes,
    route_weight,
    w_exp_gate,
    w_exp_up,
    w_exp_down,
):
    mixed = token_mixer(
        mix_query,
        forget_input,
        mix_value,
        out_gate_input,
        decay_shift,
        forget_floor,
        head_gain,
        w_mix_out,
    )
    moe_out = experts_layer(
        moe_input, moe_gain, routes, route_weight, w_exp_gate, w_exp_up, w_exp_down
    )
    return (mixed, moe_out)


def solution(mesh):
    torus = Mesh(mesh.devices.reshape(8, 4, 8, 2), ("ep_0", "ep_1", "tp_0", "tp_1"))
    placed = (
        P(EP, TP),
        P(EP, TP),
        P(EP, TP),
        P(EP, TP),
        P(EP, TP),
        P(TP),
        P(),
        P(None, TP),
        P(EP, None),
        P(),
        P(EP, None),
        P(EP, None),
        P(EP, None, TP),
        P(EP, None, TP),
        P(EP, TP, None),
    )
    return jax.shard_map(
        body, mesh=torus, in_specs=placed, out_specs=(P(EP, TP), P(EP, TP)), check_vma=False
    )
```

profile of v0, /device:TPU:1, one launch (start us, length us, event | category | flops | bytes accessed | tf_op | source)
XLA Modules:
  0.0 226.4 jit_solution(9882331451542621476)
XLA Ops:
  8.1 0.9 copy.57
  9.0 0.1 eq.29
  9.2 0.1 eq.25
  9.3 0.7 broadcast_multiply_fusion
  10.0 1.2 reduce-window.16
  11.2 0.2 slice_reduce_fusion
  11.5 0.1 copy.56
  11.6 0.1 mul.373
  11.9 2.4 %scatter_custom_fusion = s32[640]{0:T(1024)S(1)} fusion(s32[512]{0:T(512)S(1)} %bitcast.177, s32[512]{0:T(512)S(1)} %add_select_fusion, s32[]{:T(128)} %constant.34.clone.1), kind=kCustom, calls=%fused_computation.173 | custom fusion | bytes 2564 | tf_op jit(solution)/shard_map/scatter | solution.py:173
  14.3 1.5 fusion
  15.9 1.0 fusion.2
  16.9 4.1 %gather_fusion = bf16[640,2048]{1,0:T(8,128)(2,1)} fusion(bf16[256,2048]{1,0:T(8,128)(2,1)S(1)} %fusion.2, s32[1024]{0:T(1024)S(1)} %pad_clamp_fusion.1), kind=kCustom, calls=%fused_computation | custom fusion | bytes 5245440 | tf_op jit(solution)/shard_map/gather | solution.py:180
  21.0 3.8 %scatter_custom_fusion.1 = bf16[640]{0:T(1024)(128)(2,1)S(1)} fusion(s32[512]{0:T(512)S(1)} %bitcast.178, bf16[512]{0:T(512)(128)(2,1)S(1)} %broadcast.266, bf16[]{:T(256)} %constant.85.clone.1), kind=kCustom, calls=%fused_computation.177 | custom fusion | bytes 1282 | tf_op jit(solution)/shard_map/scatter | solution.py:178
  24.7 1.1 dynamic-slice_multiply_fusion
  25.9 23.5 %all_to_all.26 = bf16[32,20,128]{2,1,0:T(8,128)(2,1)S(1)} all-to-all(bf16[32,20,128]{2,1,0:T(8,128)(2,1)S(1)} %all_to_all.17), channel_id=1, replica_groups=mesh['ep_0'=8,'ep_1'=4,'tp_0'=8,'tp_1'=2] {'ep_0','ep_1'}, dimensions={0} | all-to-all | bytes 327680 | tf_op jit(solution)/shard_map/all_to_all | solution.py:186
  49.4 0.2 copy.60
  49.6 0.3 broadcast_in_dim.28
  49.9 71.8 %all_to_all.27 = bf16[16,640,128]{1,2,0:T(8,128)(2,1)S(1)} all-to-all(bf16[16,640,128]{1,2,0:T(8,128)(2,1)S(1)} %broadcast_in_dim.28), channel_id=1, replica_groups=mesh['ep_0'=8,'ep_1'=4,'tp_0'=8,'tp_1'=2] {'tp_0','tp_1'}, dimensions={0} | all-to-all | bytes 5242880 | tf_op jit(solution)/shard_map/all_to_all | solution.py:61
  121.7 1.5 copy-done.2
  123.2 0.9 fusion.7
  124.1 0.3 copy-done.13
  124.4 6.1 %fusion.3 = bf16[80,16,8,128]{3,2,1,0:T(8,128)(2,1)} fusion(bf16[1,256,2048]{2,1,0:T(8,128)(2,1)S(1)} %copy-done, bf16[640,2048]{0,1:T(8,128)(2,1)} %bitcast.175, bf16[1,2048,256]{2,1,0:T(8,128)(2,1)S(1)} %copy-done.13, f32[640,256]{1,0:T(8,128)S(1)} %fusion.7), kind=kOutput, calls=%fused_computation.11 | convolution fusion | flops 1344471040 | bytes 7995392 | tf_op jit(solution)/shard_map/dot_general | solution.py:191
  130.5 2.4 %copy.68 = bf16[80,16,8,128]{3,2,0,1:T(8,128)(2,1)S(1)} copy(bf16[80,16,8,128]{3,2,1,0:T(8,128)(2,1)} %fusion.3) | data formatting | bytes 5242880 | tf_op jit(solution)/shard_map/reshape | solution.py:79
  132.9 1.7 copy.62
  134.8 0.7 copy-done.5
  135.8 0.1 copy.52
  135.9 0.1 fusion.156
  136.1 0.1 copy.53
  136.3 0.1 copy.54
  136.4 0.2 broadcast.258
  136.8 0.2 slice_reduce_fusion.1
  137.0 0.2 fusion.93
  137.2 0.3 convolution_convert_fusion.2
  137.5 9.5 %all-gather.2 = bf16[4,129,128]{2,1,0:T(8,128)(2,1)S(1)} all-gather(bf16[1,129,128]{2,1,0:T(8,128)(2,1)S(1)} %maximum_bitcast_fusion), channel_id=2, replica_groups=mesh['ep_0'=8,'ep_1'=4,'tp_0'=8,'tp_1'=2] {'ep_1'}, dimensions={0}, use_global_device_ids=true | all-gather | bytes 165120 | tf_op jit(solution)/shard_map/all_gather | solution.py:28
  147.4 0.1 fusion.94
  147.6 19.3 %all-gather.3 = bf16[8,129,128]{2,1,0:T(8,128)(2,1)S(1)} all-gather(bf16[1,129,128]{2,1,0:T(8,128)(2,1)S(1)} %maximum_bitcast_fusion.1), channel_id=3, replica_groups=mesh['ep_0'=8,'ep_1'=4,'tp_0'=8,'tp_1'=2] {'ep_0'}, dimensions={0}, use_global_device_ids=true | all-gather | bytes 297216 | tf_op jit(solution)/shard_map/all_gather | solution.py:28
  166.8 0.4 convolution_select_fusion
  167.3 0.3 fusion.157
  167.6 0.6 multiply_reduce_fusion
  168.2 0.7 fusion.42
  169.0 17.1 %reduce-scatter.5.cloned.1.call-done = bf16[1,640,128]{2,1,0:T(8,128)(2,1)} async-done(((bf16[8,640,128]{2,1,0:T(8,128)(2,1)}), bf16[1,640,128]{2,1,0:T(8,128)(2,1)}) %reduce-scatter.5.cloned.1.call-update) | async-done | bytes 163856 | tf_op jit(solution)/shard_map/reduce_scatter | solution.py:89
  186.1 1.6 all_to_all.20
  187.7 9.9 %all-to-all-start.2 = ((bf16[32,20,128]{2,1,0:T(8,128)(2,1)}), bf16[32,20,128]{2,1,0:T(8,128)(2,1)S(1)}, u32[]{:S(2)}, u32[]{:S(2)}) async-start(bf16[32,20,128]{2,1,0:T(8,128)(2,1)} %all_to_all.20), calls=%async_computation.4 | async-start | bytes 393216 | tf_op jit(solution)/shard_map/all_to_all | solution.py:197
  197.6 0.1 copy.63
  197.8 16.4 %all-gather.6.cloned.1.call-done = bf16[256,2048]{0,1:T(8,128)(2,1)} async-done(((bf16[256,128]{0,1:T(8,128)(2,1)}), bf16[256,2048]{0,1:T(8,128)(2,1)}) %all-gather.6.cloned.1.call-update) | async-done | bytes 1048592 | tf_op jit(solution)/shard_map/all_gather | solution.py:148
  214.1 2.3 %convolution_convert_fusion.1 = bf16[256,128]{1,0:T(8,128)(2,1)} fusion(bf16[256,2048]{0,1:T(8,128)(2,1)} %all-gather.6.cloned.1.call-done, bf16[2048,128]{1,0:T(8,128)(2,1)S(1)} %copy-done.3), kind=kOutput, calls=%fused_computation.16 | convolution fusion | flops 134250496 | bytes 1638400 | tf_op jit(solution)/shard_map/dot_general | solution.py:147
  216.5 1.3 gather_fusion.1
  217.9 1.1 fusion.12
  (67 shorter events, 1.4 us)
Async XLA Ops:
  8.0 116.1 %copy-start = (bf16[1,256,2048]{2,1,0:T(8,128)(2,1)S(1)}, bf16[1,256,2048]{2,1,0:T(8,128)(2,1)}, u32[]{:S(2)}) copy-start(bf16[1,256,2048]{2,1,0:T(8,128)(2,1)} %param.29) | copy-start | bytes 3145732
  8.0 7.9 %copy-start.1 = (bf16[256,2048]{1,0:T(8,128)(2,1)S(1)}, bf16[256,2048]{1,0:T(8,128)(2,1)}, u32[]{:S(2)}) copy-start(bf16[256,2048]{1,0:T(8,128)(2,1)} %param.23) | copy-start | bytes 3145732
  8.0 139.0 %reduce-scatter.3.cloned.1.call-start = ((), (), s32[]{:S(2)}) async-start(), calls=%async_computation.6 | async-start | bytes 3932160 | tf_op jit(solution)/shard_map/reduce_scatter | solution.py:88
  49.9 73.3 %copy-start.12 = (bf16[1,2048,256]{2,1,0:T(8,128)(2,1)S(1)}, bf16[1,2048,256]{2,1,0:T(8,128)(2,1)}, u32[]{:S(2)}) copy-start(bf16[1,2048,256]{2,1,0:T(8,128)(2,1)} %param.27) | copy-start | bytes 3145732
  121.7 1.5 copy-start.2
  123.2 1.2 copy-start.13
  134.6 0.8 copy-start.5
  134.6 1.0 copy-start.10
  134.6 1.0 copy-start.9
  134.7 2.6 %copy-start.4 = (bf16[256,128]{1,0:T(8,128)(2,1)S(1)}, bf16[256,128]{1,0:T(8,128)(2,1)}, u32[]{:S(2)}) copy-start(bf16[256,128]{1,0:T(8,128)(2,1)} %param.17) | copy-start | bytes 196612
  134.7 12.4 %copy-start.6 = (bf16[256,128]{1,0:T(8,128)(2,1)S(1)}, bf16[256,128]{1,0:T(8,128)(2,1)}, u32[]{:S(2)}) copy-start(bf16[256,128]{1,0:T(8,128)(2,1)} %param.15) | copy-start | bytes 196612
  134.7 12.6 %copy-start.7 = (bf16[256,128]{1,0:T(8,128)(2,1)S(1)}, bf16[256,128]{1,0:T(8,128)(2,1)}, u32[]{:S(2)}) copy-start(bf16[256,128]{1,0:T(8,128)(2,1)} %param.18) | copy-start | bytes 196612
  134.7 51.4 %reduce-scatter.5.cloned.1.call-start = ((), (), s32[]{:S(2)}) async-start(), calls=%async_computation.7 | async-start | bytes 1474560 | tf_op jit(solution)/shard_map/reduce_scatter | solution.py:89
  137.5 30.8 %copy-start.11 = (f32[128]{0:T(128)S(1)}, f32[128]{0:T(128)}, u32[]{:S(2)}) copy-start(f32[128]{0:T(128)} %param.21) | copy-start | bytes 1540
  147.0 50.6 %copy-start.8 = (f32[256,2]{0,1:T(2,128)S(1)}, f32[256,2]{0,1:T(2,128)}, u32[]{:S(2)}) copy-start(f32[256,2]{0,1:T(2,128)} %param.26) | copy-start | bytes 6148
  147.0 67.1 %copy-start.3 = (bf16[2048,128]{1,0:T(8,128)(2,1)S(1)}, bf16[2048,128]{1,0:T(8,128)(2,1)}, u32[]{:S(2)}) copy-start(bf16[2048,128]{1,0:T(8,128)(2,1)} %param.22) | copy-start | bytes 1572868
  147.0 67.1 %all-gather.6.cloned.1.call-start = ((), (), s32[]{:S(2)}) async-start(), calls=%async_computation.5 | async-start | bytes 1114112 | tf_op jit(solution)/shard_map/all_gather | solution.py:148
  187.7 28.8 %all-to-all-start.2 = ((bf16[32,20,128]{2,1,0:T(8,128)(2,1)}), bf16[32,20,128]{2,1,0:T(8,128)(2,1)S(1)}, u32[]{:S(2)}, u32[]{:S(2)}) async-start(bf16[32,20,128]{2,1,0:T(8,128)(2,1)} %all_to_all.20), calls=%async_computation.4 | async-start | bytes 393216 | tf_op jit(solution)/shard_map/all_to_all | solution.py:197
Sparse Core Ops, SparseCore 0:
  134.8 9.7 reduce-scatter.2
  147.4 38.5 reduce-scatter.4
Sparse Core Ops, SparseCore 1:
  169.1 45.0 all-gather.5
where the time goes:
time: 227 us; the launch traced here: 226 us
  blocking collectives  124 us (55%)
  waiting for transfers between devices  33.5 us (15%)
  local copies, waits for them, and re-layouts  23.8 us (10%)
  between operations  16 us (7%)
  matrix products  11 us (5%)
  starting transfers between devices  10 us (4%)
  other arithmetic  8.08 us (4%)
    all_to_all x1, blocking collectives, sent_to_all(): lax.all_to_all(jnp.broadcast_to(shard[None], (peers, *shard.shape)), axis...  71.8 us
    all_gather x2, blocking collectives, gathered_once(): both, at, found = (lax.all_gather(jnp.concatenate(lines), axis), 0, {})  28.7 us
    all_to_all x1, blocking collectives, experts_layer(): lax.all_to_all(own_slice, EP, split_axis=0, concat_axis=0, tiled=True)  23.5 us
    reduce_scatter x1, waiting for transfers between devices, scatter_pairs(): return lax.psum_scatter(tiles, chips, scatter_dimension=0, tiled=True)[0]  17.1 us
    all_gather x1, waiting for transfers between devices, token_mixer(): lax.all_gather(head_out, TP, axis=1, tiled=True)  16.4 us
    all_to_all x1, starting transfers between devices, experts_layer(): lax.all_to_all(summed, EP, split_axis=0, concat_axis=0, tiled=True)  9.92 us
    dot_general x1, matrix products, experts_layer(): partial_value = jnp.dot(hidden, w_down, preferred_element_type=jnp.float32)  6.11 us
  transfers between devices with their start and end apart: 4, of which 2 were waited for; matrix products, arithmetic and copies ran while one was open for 3% of the time, Pallas kernels for 0%

commit v1 on v0

--- a/solution.py
+++ b/solution.py
@@ -145,7 +145,9 @@
     normed_heads = (block_result * inverse * head_gain * gated).transpose(1, 0, 2)
     head_out = normed_heads.reshape(length, heads_here * head_size).astype(jnp.bfloat16)
     mixed = jnp.dot(
-        lax.all_gather(head_out, TP, axis=1, tiled=True),
+        jnp.concatenate(
+            lax.all_to_all(jnp.stack([head_out] * lax.axis_size(TP)), TP, 0, 0), axis=1
+        ),
         w_mix_out,
         preferred_element_type=jnp.float32,
     )

time: 227 us -> 251 us (1.11); the launches traced: 226 us -> 248 us
  waiting for transfers between devices: 33.5 us -> 50.3 us
  starting transfers between devices: 10 us -> 17.4 us
    reduce_scatter x1, waiting for transfers between devices: 17.1 us -> 41.5 us  [scatter_pairs(): return lax.psum_scatter(tiles, chips, scatter_dimension=0, tiled=True)[0]]
    all_gather x1 -> x0, waiting for transfers between devices: 16.4 us -> none  [token_mixer(): lax.all_gather(head_out, TP, axis=1, tiled=True)]
    all_to_all x0 -> x1, starting transfers between devices: none -> 11.7 us  [token_mixer(): lax.all_to_all(jnp.stack([head_out] * lax.axis_size(TP)), TP, 0, 0)]
    all_to_all x1, waiting for transfers between devices: 0.01 us -> 8.68 us  [experts_layer(): lax.all_to_all(summed, EP, split_axis=0, concat_axis=0, tiled=True)]
    all_to_all x1, starting transfers between devices: 9.92 us -> 5.61 us  [experts_layer(): lax.all_to_all(summed, EP, split_axis=0, concat_axis=0, tiled=True)]
  transfers between devices with their start and end apart: 4 -> 4, of which waited for: 2 -> 2; matrix products, arithmetic and copies ran while one was open for 3% -> 2% of each run, Pallas kernels for 0% -> 0%
where the time goes in v1:
time: 251 us; the launch traced here: 248 us
  blocking collectives  124 us (49%)
  waiting for transfers between devices  50.3 us (20%)
  local copies, waits for them, and re-layouts  24.9 us (10%)
  starting transfers between devices  17.4 us (7%)
  between operations  14.6 us (6%)
  matrix products  9.74 us (4%)
  other arithmetic  7.45 us (3%)
    all_to_all x1, blocking collectives, sent_to_all(): lax.all_to_all(jnp.broadcast_to(shard[None], (peers, *shard.shape)), axis...  71.8 us
    reduce_scatter x1, waiting for transfers between devices, scatter_pairs(): return lax.psum_scatter(tiles, chips, scatter_dimension=0, tiled=True)[0]  41.5 us
    all_gather x2, blocking collectives, gathered_once(): both, at, found = (lax.all_gather(jnp.concatenate(lines), axis), 0, {})  28.2 us
    all_to_all x1, blocking collectives, experts_layer(): lax.all_to_all(own_slice, EP, split_axis=0, concat_axis=0, tiled=True)  23.5 us
    all_to_all x1, starting transfers between devices, token_mixer(): lax.all_to_all(jnp.stack([head_out] * lax.axis_size(TP)), TP, 0, 0)  11.7 us
    all_to_all x1, waiting for transfers between devices, experts_layer(): lax.all_to_all(summed, EP, split_axis=0, concat_axis=0, tiled=True)  8.68 us
    dot_general x1, matrix products, experts_layer(): partial_value = jnp.dot(hidden, w_down, preferred_element_type=jnp.float32)  6.11 us
    all_to_all x1, starting transfers between devices, experts_layer(): lax.all_to_all(summed, EP, split_axis=0, concat_axis=0, tiled=True)  5.61 us
  transfers between devices with their start and end apart: 4, of which 2 were waited for; matrix products, arithmetic and copies ran while one was open for 2% of the time, Pallas kernels for 0%

profile of v1, /device:TPU:1, one launch (start us, length us, event | category | flops | bytes accessed | tf_op | source)
XLA Modules:
  0.0 247.8 jit_solution(2324633150962991951)
XLA Ops:
  7.2 0.9 copy.58
  8.2 0.1 eq.29
  8.3 0.1 eq.25
  8.5 0.7 broadcast_multiply_fusion
  9.2 1.2 reduce-window.16
  10.4 0.2 slice_reduce_fusion
  10.6 0.1 copy.57
  10.8 0.1 mul.373
  11.0 2.4 scatter_custom_fusion
  13.5 1.5 fusion
  15.0 1.0 fusion.2
  16.0 4.1 %gather_fusion = bf16[640,2048]{1,0:T(8,128)(2,1)} fusion(bf16[256,2048]{1,0:T(8,128)(2,1)S(1)} %fusion.2, s32[1024]{0:T(1024)S(1)} %pad_clamp_fusion.1), kind=kCustom, calls=%fused_computation | custom fusion | bytes 5245440 | tf_op jit(solution)/shard_map/gather | solution.py:182
  20.1 3.8 %scatter_custom_fusion.1 = bf16[640]{0:T(1024)(128)(2,1)S(1)} fusion(s32[512]{0:T(512)S(1)} %bitcast.182, bf16[512]{0:T(512)(128)(2,1)S(1)} %broadcast.267, bf16[]{:T(256)} %constant.85.clone.1), kind=kCustom, calls=%fused_computation.177 | custom fusion | bytes 1282 | tf_op jit(solution)/shard_map/scatter | solution.py:180
  23.9 1.1 dynamic-slice_multiply_fusion
  25.0 23.5 %all_to_all.31 = bf16[32,20,128]{2,1,0:T(8,128)(2,1)S(1)} all-to-all(bf16[32,20,128]{2,1,0:T(8,128)(2,1)S(1)} %all_to_all.21), channel_id=1, replica_groups=mesh['ep_0'=8,'ep_1'=4,'tp_0'=8,'tp_1'=2] {'ep_0','ep_1'}, dimensions={0} | all-to-all | bytes 327680 | tf_op jit(solution)/shard_map/all_to_all | solution.py:188
  48.6 0.2 copy.61
  48.7 0.3 broadcast_in_dim.28
  49.0 71.8 %all_to_all.32 = bf16[16,640,128]{1,2,0:T(8,128)(2,1)S(1)} all-to-all(bf16[16,640,128]{1,2,0:T(8,128)(2,1)S(1)} %broadcast_in_dim.28), channel_id=1, replica_groups=mesh['ep_0'=8,'ep_1'=4,'tp_0'=8,'tp_1'=2] {'tp_0','tp_1'}, dimensions={0} | all-to-all | bytes 5242880 | tf_op jit(solution)/shard_map/all_to_all | solution.py:61
  120.8 1.5 copy-done.2
  122.4 0.9 fusion.7
  123.2 0.3 copy-done.13
  123.6 6.1 %fusion.3 = bf16[80,16,8,128]{3,2,1,0:T(8,128)(2,1)} fusion(bf16[1,256,2048]{2,1,0:T(8,128)(2,1)S(1)} %copy-done, bf16[640,2048]{0,1:T(8,128)(2,1)} %bitcast.179, bf16[1,2048,256]{2,1,0:T(8,128)(2,1)S(1)} %copy-done.13, f32[640,256]{1,0:T(8,128)S(1)} %fusion.7), kind=kOutput, calls=%fused_computation.11 | convolution fusion | flops 1344471040 | bytes 7995392 | tf_op jit(solution)/shard_map/dot_general | solution.py:193
  129.7 2.4 copy.69
  132.1 1.7 copy.63
  133.9 0.7 copy-done.5
  135.1 0.1 fusion.156
  135.2 0.1 copy.54
  135.4 0.1 copy.55
  135.5 0.2 broadcast.259
  136.3 0.2 slice_reduce_fusion.1
  136.4 0.2 fusion.93
  136.6 0.3 convolution_convert_fusion.2
  136.9 9.5 %all-gather.2 = bf16[4,129,128]{2,1,0:T(8,128)(2,1)S(1)} all-gather(bf16[1,129,128]{2,1,0:T(8,128)(2,1)S(1)} %maximum_bitcast_fusion), channel_id=2, replica_groups=mesh['ep_0'=8,'ep_1'=4,'tp_0'=8,'tp_1'=2] {'ep_1'}, dimensions={0}, use_global_device_ids=true | all-gather | bytes 165120 | tf_op jit(solution)/shard_map/all_gather | solution.py:28
  146.4 0.1 fusion.94
  146.6 18.8 %all-gather.3 = bf16[8,129,128]{2,1,0:T(8,128)(2,1)S(1)} all-gather(bf16[1,129,128]{2,1,0:T(8,128)(2,1)S(1)} %maximum_bitcast_fusion.1), channel_id=3, replica_groups=mesh['ep_0'=8,'ep_1'=4,'tp_0'=8,'tp_1'=2] {'ep_0'}, dimensions={0}, use_global_device_ids=true | all-gather | bytes 297216 | tf_op jit(solution)/shard_map/all_gather | solution.py:28
  165.4 0.4 convolution_select_fusion
  165.8 0.3 fusion.157
  166.2 0.6 multiply_reduce_fusion
  167.0 1.1 stack.2
  168.1 11.7 %all-to-all-start = ((bf16[16,256,128]{1,2,0:T(8,128)(2,1)}), bf16[16,256,128]{1,2,0:T(8,128)(2,1)S(1)}, u32[]{:S(2)}, u32[]{:S(2)}) async-start(bf16[16,256,128]{1,2,0:T(8,128)(2,1)} %stack.2), calls=%async_computation | async-start | bytes 2097152 | tf_op jit(solution)/shard_map/all_to_all | solution.py:149
  179.8 41.5 %reduce-scatter.5.cloned.1.call-done = bf16[1,640,128]{2,1,0:T(8,128)(2,1)} async-done(((bf16[8,640,128]{2,1,0:T(8,128)(2,1)}), bf16[1,640,128]{2,1,0:T(8,128)(2,1)}) %reduce-scatter.5.cloned.1.call-update) | async-done | bytes 163856 | tf_op jit(solution)/shard_map/reduce_scatter | solution.py:89
  221.3 1.6 all_to_all.24
  222.9 5.6 %all-to-all-start.3 = ((bf16[32,20,128]{2,1,0:T(8,128)(2,1)}), bf16[32,20,128]{2,1,0:T(8,128)(2,1)S(1)}, u32[]{:S(2)}, u32[]{:S(2)}) async-start(bf16[32,20,128]{2,1,0:T(8,128)(2,1)} %all_to_all.24), calls=%async_computation.5 | async-start | bytes 393216 | tf_op jit(solution)/shard_map/all_to_all | solution.py:199
  228.6 0.1 copy.64
  228.7 1.1 convolution_convert_fusion.1
  229.8 8.7 %all-to-all-done.3 = bf16[32,20,128]{2,1,0:T(8,128)(2,1)S(1)} async-done(((bf16[32,20,128]{2,1,0:T(8,128)(2,1)}), bf16[32,20,128]{2,1,0:T(8,128)(2,1)S(1)}, u32[]{:S(2)}, u32[]{:S(2)}) %all-to-all-start.3) | async-done | bytes 163872 | tf_op jit(solution)/shard_map/all_to_all | solution.py:199
  238.6 1.3 gather_fusion.1
  239.9 1.1 fusion.12
  (67 shorter events, 1.5 us)
Async XLA Ops:
  7.2 116.1 %copy-start = (bf16[1,256,2048]{2,1,0:T(8,128)(2,1)S(1)}, bf16[1,256,2048]{2,1,0:T(8,128)(2,1)}, u32[]{:S(2)}) copy-start(bf16[1,256,2048]{2,1,0:T(8,128)(2,1)} %param.29) | copy-start | bytes 3145732
  7.2 7.9 %copy-start.1 = (bf16[256,2048]{1,0:T(8,128)(2,1)S(1)}, bf16[256,2048]{1,0:T(8,128)(2,1)}, u32[]{:S(2)}) copy-start(bf16[256,2048]{1,0:T(8,128)(2,1)} %param.23) | copy-start | bytes 3145732
  7.2 159.0 %reduce-scatter.3.cloned.1.call-start = ((), (), s32[]{:S(2)}) async-start(), calls=%async_computation.6 | async-start | bytes 3932160 | tf_op jit(solution)/shard_map/reduce_scatter | solution.py:88
  49.0 73.3 %copy-start.12 = (bf16[1,2048,256]{2,1,0:T(8,128)(2,1)S(1)}, bf16[1,2048,256]{2,1,0:T(8,128)(2,1)}, u32[]{:S(2)}) copy-start(bf16[1,2048,256]{2,1,0:T(8,128)(2,1)} %param.27) | copy-start | bytes 3145732
  120.8 1.5 copy-start.2
  122.4 1.2 copy-start.13
  133.8 0.8 copy-start.5
  133.8 1.0 copy-start.10
  133.8 1.0 copy-start.9
  133.8 2.2 copy-start.6
  133.8 2.3 copy-start.7
  133.8 2.8 %copy-start.4 = (bf16[256,128]{1,0:T(8,128)(2,1)S(1)}, bf16[256,128]{1,0:T(8,128)(2,1)}, u32[]{:S(2)}) copy-start(bf16[256,128]{1,0:T(8,128)(2,1)} %param.17) | copy-start | bytes 196612
  133.9 87.4 %reduce-scatter.5.cloned.1.call-start = ((), (), s32[]{:S(2)}) async-start(), calls=%async_computation.7 | async-start | bytes 1474560 | tf_op jit(solution)/shard_map/reduce_scatter | solution.py:89
  136.9 29.9 %copy-start.11 = (f32[128]{0:T(128)S(1)}, f32[128]{0:T(128)}, u32[]{:S(2)}) copy-start(f32[128]{0:T(128)} %param.21) | copy-start | bytes 1540
  166.2 62.4 %copy-start.8 = (f32[256,2]{0,1:T(2,128)S(1)}, f32[256,2]{0,1:T(2,128)}, u32[]{:S(2)}) copy-start(f32[256,2]{0,1:T(2,128)} %param.26) | copy-start | bytes 6148
  166.2 62.5 %copy-start.3 = (bf16[2048,128]{1,0:T(8,128)(2,1)S(1)}, bf16[2048,128]{1,0:T(8,128)(2,1)}, u32[]{:S(2)}) copy-start(bf16[2048,128]{1,0:T(8,128)(2,1)} %param.22) | copy-start | bytes 1572868
  168.1 54.9 %all-to-all-start = ((bf16[16,256,128]{1,2,0:T(8,128)(2,1)}), bf16[16,256,128]{1,2,0:T(8,128)(2,1)S(1)}, u32[]{:S(2)}, u32[]{:S(2)}) async-start(bf16[16,256,128]{1,2,0:T(8,128)(2,1)} %stack.2), calls=%async_computation | async-start | bytes 2097152 | tf_op jit(solution)/shard_map/all_to_all | solution.py:149
  222.9 15.6 %all-to-all-start.3 = ((bf16[32,20,128]{2,1,0:T(8,128)(2,1)}), bf16[32,20,128]{2,1,0:T(8,128)(2,1)S(1)}, u32[]{:S(2)}, u32[]{:S(2)}) async-start(bf16[32,20,128]{2,1,0:T(8,128)(2,1)} %all_to_all.24), calls=%async_computation.5 | async-start | bytes 393216 | tf_op jit(solution)/shard_map/all_to_all | solution.py:199
Sparse Core Ops, SparseCore 0:
  134.0 9.7 reduce-scatter.2
  166.3 54.9 reduce-scatter.4
